TPU v7x, 512 devices: a whole 4x4x16 slice. The times are simulated.
512 devices in a mesh: ep: 32 (over z, core), tp: 16 (over y, x).
Axes of the slice: x: 4, y: 4, z: 16, core: 2. Of those that a mesh axis runs over, the one named last changes fastest.
Arguments:
- query_rows: bfloat16 [12288, 2048], P('ep', 'tp'), may hold values from -6 to 6
- key_rows: bfloat16 [12288, 2048], P('ep', 'tp'), may hold values from -6 to 6
- value_rows: bfloat16 [12288, 2048], P('ep', 'tp'), may hold values from -6 to 6
- second_scale: float32 [16], P('tp'), may hold values from 0.3 to 0.8
- head_gain: float32 [128], replicated, may hold values from 0.1 to 1.9
- out_weight: bfloat16 [2048, 4096], P(None, 'tp'), may hold values from -0.125 to 0.125
- routed_rows: bfloat16 [4096, 4096], P('ep', 'tp'), may hold values from -6 to 6
- norm_gain: float32 [4096], replicated, may hold values from 0.1 to 1.9
- route_ids: int32 [4096, 2], P('ep'), may hold values from 0 to 31, all different within a row; in each aligned block of 128 rows (0 to 127, 128 to 255, ...) at most 16 rows name the same one
- route_weight: float32 [4096, 2], P('ep'), may hold values from 0.1 to 0.9
- expert_gate: bfloat16 [32, 4096, 2048], P('ep', None, 'tp'), may hold values from -0.09375 to 0.09375
- expert_up: bfloat16 [32, 4096, 2048], P('ep', None, 'tp'), may hold values from -0.09375 to 0.09375
- expert_down: bfloat16 [32, 2048, 4096], P('ep', None, 'tp'), may hold values from -0.125 to 0.125
Outputs:
- mixer_out: bfloat16 [12288, 4096], P('ep', 'tp')
- expert_mix: bfloat16 [4096, 4096], P('ep', 'tp')
Inputs may be any that keep to these rules, and one draw needn't show every extreme that they name: `route_ids`: among the 128 tokens of one index of ep, no expert is named by more than 16 of them, a bound that some block reaches.
All inputs are finite; a program needn't handle non-finite values.
Results may differ from a plain program's by a relative error of at most 0.0085.
Values may be sent and summed in bfloat16 or wider, within the bound.
A program may use at most 64 MiB of HBM per device.

v0:
```python
import jax
import jax.numpy as jnp
from jax import lax
from jax.sharding import PartitionSpec as P

eps = 1e-06
head_factor = 0.8
neg_big = -1e30
key_block_rows = 1024


def side_by_side(arrays, axis, dim, along):
    both = jnp.concatenate(arrays, axis=along)
    result, at, finished = (lax.all_gather(both, axis, axis=dim, tiled=True), 0, [])
    for a in arrays:
        finished.append(lax.slice_in_dim(result, at, at + a.shape[along], axis=along))
        at += a.shape[along]
    return tuple(finished)


def rms_rows(rows_in, gain):
    floats = rows_in.astype(jnp.float32)
    factor = lax.rsqrt(jnp.mean(floats * floats, axis=-1, keepdims=True) + eps)
    return (floats * factor * gain).astype(jnp.bfloat16)


def per_device(
    query_rows,
    key_rows,
    value_rows,
    second_scale,
    head_gain,
    out_weight,
    routed_rows,
    norm_gain,
    route_ids,
    route_weight,
    expert_gate,
    expert_up,
    expert_down,
):
    count_a = query_rows.shape[0]
    per_head = second_scale.shape[0]
    head_dim = query_rows.shape[1] // (2 * per_head)
    value_dim = head_gain.shape[0]
    query_four = query_rows.reshape(count_a, per_head, 2, head_dim)
    query_pos = lax.axis_index("ep") * count_a + jnp.arange(count_a, dtype=jnp.int32)

    def key_block(carry_state, key_part, value_part, block_start):
        key_count = key_part.shape[0]
        key_four = key_part.reshape(key_count, per_head, 2, head_dim)
        value_three = value_part.reshape(key_count, per_head, value_dim)
        scores = jnp.einsum(
            "ihcd,jhcd->ihcj", query_four, key_four, preferred_element_type=jnp.float32
        ) * head_dim ** (-0.5)
        allowed = (
            query_pos[:, None] >= block_start + jnp.arange(key_count, dtype=jnp.int32)[None, :]
        )[:, None, None, :]
        scores = jnp.where(allowed, scores, neg_big)
        old_max, old_sum, old_acc = carry_state
        new_max = jnp.maximum(old_max, jnp.max(scores, axis=-1))
        weights = jnp.where(allowed, jnp.exp(scores - new_max[..., None]), 0.0)
        shrink = jnp.exp(old_max - new_max)
        new_sum = old_sum * shrink + jnp.sum(weights, axis=-1)
        update = jnp.einsum(
            "ihcj,jhe->ihce",
            weights.astype(jnp.bfloat16),
            value_three,
            preferred_element_type=jnp.float32,
        )
        return (new_max, new_sum, old_acc * shrink[..., None] + update)

    start_state = (
        jnp.full((count_a, per_head, 2), neg_big, jnp.float32),
        jnp.zeros((count_a, per_head, 2), jnp.float32),
        jnp.zeros((count_a, per_head, 2, value_dim), jnp.float32),
    )
    key_part, value_part = side_by_side((key_rows, value_rows), "ep", 0, 1)
    key_count = key_part.shape[0]

    def step_block(block_num, inner_state):
        offset_rows = block_num * key_block_rows
        key_slice = lax.dynamic_slice_in_dim(key_part, offset_rows, key_block_rows, 0)
        value_slice = lax.dynamic_slice_in_dim(value_part, offset_rows, key_block_rows, 0)
        return key_block(inner_state, key_slice, value_slice, offset_rows)

    run_max, run_sum, run_acc = lax.fori_loop(
        0, key_count // key_block_rows, step_block, start_state
    )
    maps_both = run_acc / run_sum[..., None]
    mixed_maps = maps_both[:, :, 0] - second_scale[None, :, None] * maps_both[:, :, 1]
    mean_sq = jnp.mean(mixed_maps * mixed_maps, axis=-1, keepdims=True)
    head_out = (
        (mixed_maps * lax.rsqrt(mean_sq + eps) * head_gain * head_factor)
        .astype(jnp.bfloat16)
        .reshape(count_a, per_head * value_dim)
    )
    count_b = routed_rows.shape[0]
    route_count = route_ids.shape[1]
    experts_here = expert_gate.shape[0]
    ep_devices = lax.axis_size("ep")
    expert_total = experts_here * ep_devices
    capacity = 2 * count_b * route_count // expert_total
    flat_expert = route_ids.reshape(-1)
    chosen = (flat_expert[:, None] == jnp.arange(expert_total, dtype=jnp.int32)[None, :]).astype(
        jnp.int32
    )
    ranks = jnp.sum((jnp.cumsum(chosen, axis=0) - 1) * chosen, axis=1)
    slot_of = flat_expert * capacity + ranks
    token_of = jnp.arange(count_b * route_count, dtype=jnp.int32) // route_count
    slot_token = jnp.full((expert_total * capacity,), count_b, jnp.int32).at[slot_of].set(token_of)
    padded = jnp.concatenate(
        [routed_rows, jnp.zeros((1, routed_rows.shape[1]), jnp.bfloat16)], axis=0
    )
    outgoing = padded[slot_token].reshape(ep_devices, experts_here, capacity, routed_rows.shape[1])
    column_parts = lax.all_to_all(outgoing, "ep", split_axis=0, concat_axis=0, tiled=True)
    arrived = rms_rows(lax.all_gather(column_parts, "tp", axis=3, tiled=True), norm_gain)
    gate_val = jnp.einsum(
        "sxcd,xdf->sxcf", arrived, expert_gate, preferred_element_type=jnp.float32
    )
    up_val = jnp.einsum("sxcd,xdf->sxcf", arrived, expert_up, preferred_element_type=jnp.float32)
    hidden = (jax.nn.silu(gate_val) * up_val).astype(jnp.bfloat16)
    weight_rows = out_weight
    attn_total = jnp.dot(
        lax.all_gather(
            head_out.reshape(1, 1, count_a, head_out.shape[1]), "tp", axis=3, tiled=True
        )[0, 0],
        weight_rows,
        preferred_element_type=jnp.float32,
    )
    weight_rows = expert_down
    moe_total = jnp.einsum(
        "sxcf,xfd->sxcd",
        lax.all_gather(hidden, "tp", axis=3, tiled=True),
        weight_rows,
        preferred_element_type=jnp.float32,
    )
    mixer_out = attn_total.astype(jnp.bfloat16)
    returned = lax.all_to_all(
        moe_total.astype(jnp.bfloat16), "ep", split_axis=0, concat_axis=0, tiled=True
    )
    flat_back = returned.reshape(expert_total * capacity, returned.shape[3])
    picked = flat_back[slot_of].astype(jnp.float32).reshape(count_b, route_count, returned.shape[3])
    expert_mix = jnp.sum(picked * route_weight[:, :, None], axis=1).astype(jnp.bfloat16)
    return (mixer_out, expert_mix)


def solution(mesh):
    placed = (
        P("ep", "tp"),
        P("ep", "tp"),
        P("ep", "tp"),
        P("tp"),
        P(),
        P(None, "tp"),
        P("ep", "tp"),
        P(),
        P("ep", None),
        P("ep", None),
        P("ep", None, "tp"),
        P("ep", None, "tp"),
        P("ep", None, "tp"),
    )
    return jax.shard_map(
        per_device,
        mesh=mesh,
        in_specs=placed,
        out_specs=(P("ep", "tp"), P("ep", "tp")),
        check_vma=False,
    )
```

profile of v0, /device:TPU:32, one launch (start us, length us, event | category | flops | bytes accessed | tf_op | source)
XLA Modules:
  0.0 361.6 jit_solution(12429718926275836795)
XLA Ops:
  14.6 36.4 %all_to_all.10 = bf16[32,1,16,256]{3,2,1,0:T(8,128)(2,1)} all-to-all(bf16[32,1,16,256]{3,2,1,0:T(8,128)(2,1)S(1)} %bitcast.173), channel_id=1, replica_groups=mesh['ep'=32,'tp'=16] {'ep'}, dimensions={0} | all-to-all | bytes 524288 | tf_op jit(solution)/shard_map/all_to_all | solution.py:116
  52.9 63.2 %all-gather.9.cloned.1.call-done = bf16[32,1,16,4096]{3,2,1,0:T(8,128)(2,1)} async-done(((bf16[32,1,16,256]{3,2,1,0:T(8,128)(2,1)}), bf16[32,1,16,4096]{3,2,1,0:T(8,128)(2,1)}) %all-gather.9.cloned.1.call-update) | async-done | bytes 4194320 | tf_op jit(solution)/shard_map/all_gather | solution.py:117
  116.0 3.2 fusion.24
  122.8 71.9 %all-gather.5.cloned.1.call-done = bf16[12288,256]{0,1:T(8,128)(2,1)} async-done(((bf16[384,256]{0,1:T(8,128)(2,1)}), bf16[12288,256]{0,1:T(8,128)(2,1)}) %all-gather.5.cloned.1.call-update) | async-done | bytes 6291472 | tf_op jit(solution)/shard_map/all_gather | solution.py:14
  194.7 6.2 %fusion.69 = (bf16[12288,128]{0,1:T(8,128)(2,1)}, bf16[12288,128]{0,1:T(8,128)(2,1)}) fusion(bf16[12288,256]{0,1:T(8,128)(2,1)} %all-gather.5.cloned.1.call-done), kind=kLoop, calls=%fused_computation.86 | loop fusion | bytes 12582912 | tf_op jit(solution)/shard_map/slice | solution.py:16
  200.9 94.7 %while.18 = (s32[]{:T(128)}, f32[384,1,2]{0,2,1:T(2,128)S(1)}, f32[384,1,2]{0,2,1:T(2,128)S(1)}, f32[384,1,2,128]{0,3,2,1:T(8,128)S(1)}, bf16[12288,128]{0,1:T(8...) while((s32[]{:T(128)}, f32[384,1,2]{0,2,1:T(2,128)S(1)}, ...), condition=%wide.region_3.4_spmd.clone, body=%wide.region_0.3_spmd.clone.sunk | while | flops 312907648 | bytes 25586904 | solution.py:87
  204.6 3.2 fusion.85
  212.5 3.2 fusion.85
  220.4 3.2 fusion.85
  228.3 3.2 fusion.85
  236.2 3.2 fusion.85
  241.6 2.4 fusion.82
  244.1 3.2 fusion.85
  252.0 3.3 fusion.85
  259.9 3.2 fusion.85
  267.8 3.2 fusion.85
  275.7 3.2 fusion.85
  283.6 3.2 fusion.85
  291.5 3.2 fusion.85
  296.5 3.1 fusion.48
  299.6 8.2 %all-to-all-start.1 = ((bf16[32,1,16,256]{3,2,1,0:T(8,128)(2,1)}), bf16[32,1,16,256]{3,2,1,0:T(8,128)(2,1)S(1)}, u32[]{:S(2)}, u32[]{:S(2)}) async-start(bf16[32,1,16,256]{3,2,1,0:T(8,128)(2,1)} %fusion.48), calls=%async_computation.1 | async-start | bytes 524288 | tf_op jit(solution)/shard_map/all_to_all | solution.py:139
  308.0 20.8 %all-to-all-done.1 = bf16[32,1,16,256]{3,2,1,0:T(8,128)(2,1)S(1)} async-done(((bf16[32,1,16,256]{3,2,1,0:T(8,128)(2,1)}), bf16[32,1,16,256]{3,2,1,0:T(8,128)(2,1)S(1)}, u32[]{:S(2)}, u32[]{:S(2)}) %all-to-all-start.1) | async-done | bytes 262176 | tf_op jit(solution)/shard_map/all_to_all | solution.py:139
  331.1 21.2 %all-gather.7.cloned.1.call-done = bf16[1,1,384,2048]{2,3,1,0:T(8,128)(2,1)} async-done(((bf16[1,1,384,128]{2,3,1,0:T(8,128)(2,1)}), bf16[1,1,384,2048]{2,3,1,0:T(8,128)(2,1)}) %all-gather.7.cloned.1.call-update) | async-done | bytes 1572880 | tf_op jit(solution)/shard_map/all_gather | solution.py:125
  352.4 2.7 fusion.39
  (200 shorter events, 67.8 us)
Async XLA Ops:
  7.2 289.4 %copy-start = (bf16[1,2048,256]{2,1,0:T(8,128)(2,1)S(1)}, bf16[1,2048,256]{2,1,0:T(8,128)(2,1)}, u32[]{:S(2)}) copy-start(bf16[1,2048,256]{2,1,0:T(8,128)(2,1)} %param.27) | copy-start | bytes 3145732
  7.2 43.8 %copy-start.4 = (bf16[384,128]{1,0:T(8,128)(2,1)S(1)}, bf16[384,128]{1,0:T(8,128)(2,1)}, u32[]{:S(2)}) copy-start(bf16[384,128]{1,0:T(8,128)(2,1)} %param.16) | copy-start | bytes 294916
  7.2 43.9 %copy-start.5 = (bf16[384,128]{1,0:T(8,128)(2,1)S(1)}, bf16[384,128]{1,0:T(8,128)(2,1)}, u32[]{:S(2)}) copy-start(bf16[384,128]{1,0:T(8,128)(2,1)} %param.17) | copy-start | bytes 294916
  7.2 44.9 %copy-start.6 = (bf16[384,128]{1,0:T(8,128)(2,1)S(1)}, bf16[384,128]{1,0:T(8,128)(2,1)}, u32[]{:S(2)}) copy-start(bf16[384,128]{1,0:T(8,128)(2,1)} %param.15) | copy-start | bytes 294916
  7.2 108.8 %all-gather.9.cloned.1.call-start = ((), (), s32[]{:S(2)}) async-start(), calls=%async_computation.4 | async-start | bytes 4456448 | tf_op jit(solution)/shard_map/all_gather | solution.py:117
  14.5 104.7 %copy-start.9 = (bf16[1,4096,128]{2,1,0:T(8,128)(2,1)S(1)}, bf16[1,4096,128]{2,1,0:T(8,128)(2,1)}, u32[]{:S(2)}) copy-start(bf16[1,4096,128]{2,1,0:T(8,128)(2,1)} %param.25) | copy-start | bytes 3145732
  14.5 104.7 %copy-start.11 = (f32[4096]{0:T(1024)S(1)}, f32[4096]{0:T(1024)}, u32[]{:S(2)}) copy-start(f32[4096]{0:T(1024)} %param.22) | copy-start | bytes 49156
  50.9 143.8 %all-gather.5.cloned.1.call-start = ((), (), s32[]{:S(2)}) async-start(), calls=%async_computation.2 | async-start | bytes 6488064 | tf_op jit(solution)/shard_map/all_gather | solution.py:14
  52.0 244.5 %all-gather.11.cloned.1.call-start = ((), (), s32[]{:S(2)}) async-start(), calls=%async_computation.5 | async-start | bytes 2228224 | tf_op jit(solution)/shard_map/all_gather | solution.py:134
  116.0 3.4 copy-start.2
  122.8 229.6 %all-gather.7.cloned.1.call-start = ((), (), s32[]{:S(2)}) async-start(), calls=%async_computation.3 | async-start | bytes 1671168 | tf_op jit(solution)/shard_map/all_gather | solution.py:125
  200.9 94.8 %copy-start.8 = (f32[128]{0:T(128)S(1)}, f32[128]{0:T(128)}, u32[]{:S(2)}) copy-start(f32[128]{0:T(128)} %param.19) | copy-start | bytes 1540
  212.5 3.3 copy-start.1
  220.4 3.3 copy-start.1
  228.3 3.3 copy-start.1
  236.2 3.3 copy-start.1
  252.0 3.3 copy-start.1
  267.8 3.3 copy-start.1
  275.7 3.3 copy-start.1
  283.6 3.3 copy-start.1
  291.5 3.3 copy-start.1
  295.6 12.3 %copy-start.7 = (f32[128,2]{0,1:T(2,128)S(1)}, f32[128,2]{0,1:T(2,128)}, u32[]{:S(2)}) copy-start(f32[128,2]{0,1:T(2,128)} %param.24) | copy-start | bytes 3076
  296.5 55.9 %copy-start.3 = (bf16[2048,256]{1,0:T(8,128)(2,1)S(1)}, bf16[2048,256]{1,0:T(8,128)(2,1)}, u32[]{:S(2)}) copy-start(bf16[2048,256]{1,0:T(8,128)(2,1)} %param.20) | copy-start | bytes 3145732
  299.6 29.2 %all-to-all-start.1 = ((bf16[32,1,16,256]{3,2,1,0:T(8,128)(2,1)}), bf16[32,1,16,256]{3,2,1,0:T(8,128)(2,1)S(1)}, u32[]{:S(2)}, u32[]{:S(2)}) async-start(bf16[32,1,16,256]{3,2,1,0:T(8,128)(2,1)} %fusion.48), calls=%async_computation.1 | async-start | bytes 524288 | tf_op jit(solution)/shard_map/all_to_all | solution.py:139
  (4 other events, 11.1 us)
Sparse Core Ops, SparseCore 0:
  51.1 64.9 all-gather.8
  118.7 75.9 all-gather.4
  197.7 59.0 all-gather.10
  296.6 55.7 all-gather.6
where the time goes:
time: 362 us
  waiting for transfers between devices  177 us (49%)
  matrix products  77 us (21%)
  blocking collectives  36.4 us (10%)
  local copies, waits for them, and re-layouts  25.7 us (7%)
  other arithmetic  21.3 us (6%)
  between operations  14.7 us (4%)
  starting transfers between devices  8.4 us (2%)
    all_gather x1, waiting for transfers between devices, side_by_side(): lax.all_gather(both, axis, axis=dim, tiled=True)  71.9 us
    all_gather x1, waiting for transfers between devices, per_device(): lax.all_gather(column_parts, 'tp', axis=3, tiled=True)  63.2 us
    dot_general x12, matrix products, key_block(): jnp.einsum('ihcj,jhe->ihce', weights.astype(jnp.bfloat16), value_three, p...  38.8 us
    all_to_all x1, blocking collectives, per_device(): lax.all_to_all(outgoing, 'ep', split_axis=0, concat_axis=0, tiled=True)  36.4 us
    dot_general x12, matrix products, key_block(): jnp.einsum('ihcd,jhcd->ihcj', query_four, key_four, preferred_element_typ...  29.1 us
    all_gather x1, waiting for transfers between devices, per_device(): lax.all_gather(head_out.reshape(1, 1, count_a, head_out.shape[1]), 'tp',...  21.2 us
    all_to_all x1, waiting for transfers between devices, per_device(): lax.all_to_all(moe_total.astype(jnp.bfloat16), 'ep', split_axis=0, concat...  20.8 us
    dynamic_slice x12, local copies, waits for them, and re-layouts, step_block(): lax.dynamic_slice_in_dim(key_part, offset_rows, key_block_rows, 0)  11.7 us
  transfers between devices with their start and end apart: 5, of which 4 were waited for; matrix products, arithmetic and copies ran while one was open for 31% of the time, Pallas kernels for 0%

commit v1 on v0

--- a/solution.py
+++ b/solution.py
@@ -1,3 +1,4 @@
+import functools
 import jax
 import jax.numpy as jnp
 from jax import lax
@@ -7,6 +8,32 @@
 head_factor = 0.8
 neg_big = -1e30
 key_block_rows = 1024
+
+
+def _wait_cube(inner_x, shard_axis):
+    side_arr = lax.axis_index(shard_axis)
+    extra = lax.axis_size(shard_axis)
+    opened, everything, left_arr = (extra, side_arr, inner_x.shape[3])
+    stack_in = [(ii, (ii + 1) % opened) for ii in range(opened)]
+    table = [(ii, (ii - 1) % opened) for ii in range(opened)]
+    outer = jnp.zeros((*inner_x.shape[:3], opened * left_arr, *inner_x.shape[4:]), inner_x.dtype)
+    out_arr = local_part = inner_x
+    p_next = opened // 2
+    outer = lax.dynamic_update_slice_in_dim(outer, inner_x, everything * left_arr, axis=3)
+    for p in range(1, p_next + 1):
+        out_arr = lax.ppermute(out_arr, shard_axis, perm=stack_in)
+        outer = lax.dynamic_update_slice_in_dim(
+            outer, out_arr, (everything - p) % opened * left_arr, axis=3
+        )
+        if p < opened - p_next:
+            local_part = lax.ppermute(local_part, shard_axis, table)
+            outer = lax.dynamic_update_slice_in_dim(
+                outer, local_part, (everything + p) % opened * left_arr, axis=3
+            )
+    return outer
+
+
+_close_edges = functools.partial(_wait_cube, shard_axis="tp")
 
 
 def side_by_side(arrays, axis, dim, along):
@@ -114,7 +141,7 @@
     )
     outgoing = padded[slot_token].reshape(ep_devices, experts_here, capacity, routed_rows.shape[1])
     column_parts = lax.all_to_all(outgoing, "ep", split_axis=0, concat_axis=0, tiled=True)
-    arrived = rms_rows(lax.all_gather(column_parts, "tp", axis=3, tiled=True), norm_gain)
+    arrived = rms_rows(_close_edges(column_parts), norm_gain)
     gate_val = jnp.einsum(
         "sxcd,xdf->sxcf", arrived, expert_gate, preferred_element_type=jnp.float32
     )

time: 362 us -> 317 us (0.88)
  waiting for transfers between devices: 177 us -> 63.1 us
  starting transfers between devices: 8.4 us -> 72.4 us
    all_gather x1, waiting for transfers between devices: 71.9 us -> 0.02 us  [side_by_side(): lax.all_gather(both, axis, axis=dim, tiled=True)]
    ppermute x0 -> x15, starting transfers between devices: none -> 66.2 us  [the longest x7 49.6 us: _wait_cube(): local_part = lax.ppermute(local_part, shard_axis, table)]
    all_gather x1 -> x0, waiting for transfers between devices: 63.2 us -> none  [per_device(): lax.all_gather(column_parts, 'tp', axis=3, tiled=True)]
    ppermute x0 -> x15, waiting for transfers between devices: none -> 25.9 us  [the longest x8 25.8 us: _wait_cube(): out_arr = lax.ppermute(out_arr, shard_axis, perm=stack_in)]
    all_gather x1, waiting for transfers between devices: 21.2 us -> 16.2 us  [per_device(): lax.all_gather(head_out.reshape(1, 1, count_a, head_out.shape[1]), 'tp',...]
  transfers between devices with their start and end apart: 5 -> 19, of which waited for: 4 -> 10; matrix products, arithmetic and copies ran while one was open for 31% -> 38% of each run, Pallas kernels for 0% -> 0%
where the time goes in v1:
time: 317 us; the launch traced here: 315 us
  matrix products  76.8 us (24%)
  starting transfers between devices  72.4 us (23%)
  waiting for transfers between devices  63.1 us (20%)
  blocking collectives  39.7 us (13%)
  local copies, waits for them, and re-layouts  28.3 us (9%)
  other arithmetic  18.9 us (6%)
  between operations  15.3 us (5%)
    ppermute x7, starting transfers between devices, _wait_cube(): local_part = lax.ppermute(local_part, shard_axis, table)  49.6 us
    all_to_all x1, blocking collectives, per_device(): lax.all_to_all(outgoing, 'ep', split_axis=0, concat_axis=0, tiled=True)  39.7 us
    dot_general x12, matrix products, key_block(): jnp.einsum('ihcj,jhe->ihce', weights.astype(jnp.bfloat16), value_three, p...  39 us
    dot_general x12, matrix products, key_block(): jnp.einsum('ihcd,jhcd->ihcj', query_four, key_four, preferred_element_typ...  28.8 us
    ppermute x8, waiting for transfers between devices, _wait_cube(): out_arr = lax.ppermute(out_arr, shard_axis, perm=stack_in)  25.8 us
    all_to_all x1, waiting for transfers between devices, per_device(): lax.all_to_all(moe_total.astype(jnp.bfloat16), 'ep', split_axis=0, concat...  21 us
    ppermute x8, starting transfers between devices, _wait_cube(): out_arr = lax.ppermute(out_arr, shard_axis, perm=stack_in)  16.7 us
    all_gather x1, waiting for transfers between devices, per_device(): lax.all_gather(head_out.reshape(1, 1, count_a, head_out.shape[1]), 'tp',...  16.2 us
  transfers between devices with their start and end apart: 19, of which 10 were waited for; matrix products, arithmetic and copies ran while one was open for 38% of the time, Pallas kernels for 0%

profile of v1, /device:TPU:32, one launch (start us, length us, event | category | flops | bytes accessed | tf_op | source)
XLA Modules:
  0.0 315.4 jit_solution(5394262396421483700)
XLA Ops:
  17.3 39.7 %all_to_all.10 = bf16[32,1,16,256]{3,2,1,0:T(8,128)(2,1)S(1)} all-to-all(bf16[32,1,16,256]{3,2,1,0:T(8,128)(2,1)S(1)} %bitcast.201), channel_id=1, replica_groups=mesh['ep'=32,'tp'=16] {'ep'}, dimensions={0} | all-to-all | bytes 524288 | tf_op jit(solution)/shard_map/all_to_all | solution.py:143
  57.0 3.3 %collective-permute-start = (bf16[32,1,16,256]{3,2,1,0:T(8,128)(2,1)S(1)}, bf16[32,1,16,256]{3,2,1,0:T(8,128)(2,1)S(1)}, u32[]{:S(2)}, u32[]{:S(2)}) collective-permute-start(bf16[32,1,16,256]{3,2,1,0:T(8,128)(2,1)S(1)} %all_to_all.10), channel_id=1, source_target_pairs={{0,1},{1,2},{2,3},{3,4},{4,5},{5,6},{6,7},{7,8},{8,9},{9,10},{10,1... | collective-permute-start | bytes 786440 | tf_op jit(solution)/shard_map/ppermute | solution.py:24
  60.4 5.8 %collective-permute-start.1 = (bf16[32,1,16,256]{3,2,1,0:T(8,128)(2,1)S(1)}, bf16[32,1,16,256]{3,2,1,0:T(8,128)(2,1)S(1)}, u32[]{:S(2)}, u32[]{:S(2)}) collective-permute-start(bf16[32,1,16,256]{3,2,1,0:T(8,128)(2,1)S(1)} %all_to_all.10), channel_id=1, source_target_pairs={{0,15},{1,0},{2,1},{3,2},{4,3},{5,4},{6,5},{7,6},{8,7},{9,8},{10,9... | collective-permute-start | bytes 786440 | tf_op jit(solution)/shard_map/ppermute | solution.py:29
  71.0 7.2 %collective-permute-start.3 = (bf16[32,1,16,256]{3,2,1,0:T(8,128)(2,1)S(1)}, bf16[32,1,16,256]{3,2,1,0:T(8,128)(2,1)S(1)}, u32[]{:S(2)}, u32[]{:S(2)}) collective-permute-start(bf16[32,1,16,256]{3,2,1,0:T(8,128)(2,1)S(1)} %collective-permute-done.1), channel_id=1, source_target_pairs={{0,15},{1,0},{2,1},{3,2},{4,3},{5,4},{6,5},{7,6},{8,7},{9,8},{10,9... | collective-permute-start | bytes 786440 | tf_op jit(solution)/shard_map/ppermute | solution.py:29
  82.6 7.2 %collective-permute-start.5 = (bf16[32,1,16,256]{3,2,1,0:T(8,128)(2,1)S(1)}, bf16[32,1,16,256]{3,2,1,0:T(8,128)(2,1)S(1)}, u32[]{:S(2)}, u32[]{:S(2)}) collective-permute-start(bf16[32,1,16,256]{3,2,1,0:T(8,128)(2,1)S(1)} %collective-permute-done.3), channel_id=1, source_target_pairs={{0,15},{1,0},{2,1},{3,2},{4,3},{5,4},{6,5},{7,6},{8,7},{9,8},{10,9... | collective-permute-start | bytes 786440 | tf_op jit(solution)/shard_map/ppermute | solution.py:29
  94.2 7.2 %collective-permute-start.7 = (bf16[32,1,16,256]{3,2,1,0:T(8,128)(2,1)S(1)}, bf16[32,1,16,256]{3,2,1,0:T(8,128)(2,1)S(1)}, u32[]{:S(2)}, u32[]{:S(2)}) collective-permute-start(bf16[32,1,16,256]{3,2,1,0:T(8,128)(2,1)S(1)} %collective-permute-done.5), channel_id=1, source_target_pairs={{0,15},{1,0},{2,1},{3,2},{4,3},{5,4},{6,5},{7,6},{8,7},{9,8},{10,9... | collective-permute-start | bytes 786440 | tf_op jit(solution)/shard_map/ppermute | solution.py:29
  105.8 7.2 %collective-permute-start.9 = (bf16[32,1,16,256]{3,2,1,0:T(8,128)(2,1)S(1)}, bf16[32,1,16,256]{3,2,1,0:T(8,128)(2,1)S(1)}, u32[]{:S(2)}, u32[]{:S(2)}) collective-permute-start(bf16[32,1,16,256]{3,2,1,0:T(8,128)(2,1)S(1)} %collective-permute-done.7), channel_id=1, source_target_pairs={{0,15},{1,0},{2,1},{3,2},{4,3},{5,4},{6,5},{7,6},{8,7},{9,8},{10,9... | collective-permute-start | bytes 786440 | tf_op jit(solution)/shard_map/ppermute | solution.py:29
  117.3 7.2 %collective-permute-start.11 = (bf16[32,1,16,256]{3,2,1,0:T(8,128)(2,1)S(1)}, bf16[32,1,16,256]{3,2,1,0:T(8,128)(2,1)S(1)}, u32[]{:S(2)}, u32[]{:S(2)}) collective-permute-start(bf16[32,1,16,256]{3,2,1,0:T(8,128)(2,1)S(1)} %collective-permute-done.9), channel_id=1, source_target_pairs={{0,15},{1,0},{2,1},{3,2},{4,3},{5,4},{6,5},{7,6},{8,7},{9,8},{10,9... | collective-permute-start | bytes 786440 | tf_op jit(solution)/shard_map/ppermute | solution.py:29
  129.1 7.5 %collective-permute-start.13 = (bf16[32,1,16,256]{3,2,1,0:T(8,128)(2,1)S(1)}, bf16[32,1,16,256]{3,2,1,0:T(8,128)(2,1)S(1)}, u32[]{:S(2)}, u32[]{:S(2)}) collective-permute-start(bf16[32,1,16,256]{3,2,1,0:T(8,128)(2,1)S(1)} %collective-permute-done.11), channel_id=1, source_target_pairs={{0,15},{1,0},{2,1},{3,2},{4,3},{5,4},{6,5},{7,6},{8,7},{9,8},{10,9... | collective-permute-start | bytes 786440 | tf_op jit(solution)/shard_map/ppermute | solution.py:29
  136.7 3.3 %collective-permute-done.12 = bf16[32,1,16,256]{3,2,1,0:T(8,128)(2,1)S(1)} collective-permute-done((bf16[32,1,16,256]{3,2,1,0:T(8,128)(2,1)S(1)}, bf16[32,1,16,256]{3,2,1,0:T(8,128)(2,1)S(1)}, u32[]{:S(2)}, u32[]{:S(2)}) %collective-permute-start.12) | collective-permute-done | bytes 262176 | tf_op jit(solution)/shard_map/ppermute | solution.py:24
  142.0 9.6 %collective-permute-done.14 = bf16[32,1,16,256]{3,2,1,0:T(8,128)(2,1)S(1)} collective-permute-done((bf16[32,1,16,256]{3,2,1,0:T(8,128)(2,1)S(1)}, bf16[32,1,16,256]{3,2,1,0:T(8,128)(2,1)S(1)}, u32[]{:S(2)}, u32[]{:S(2)}) %collective-permute-start.14) | collective-permute-done | bytes 262176 | tf_op jit(solution)/shard_map/ppermute | solution.py:24
  156.1 6.2 %fusion.63 = (bf16[12288,128]{0,1:T(8,128)(2,1)}, bf16[12288,128]{0,1:T(8,128)(2,1)}) fusion(bf16[12288,256]{0,1:T(8,128)(2,1)} %all-gather.4.cloned.1.call-done), kind=kLoop, calls=%fused_computation.101 | loop fusion | bytes 12582912 | tf_op jit(solution)/shard_map/slice | solution.py:43
  162.3 94.5 %while.18 = (s32[]{:T(128)}, f32[384,1,2]{0,2,1:T(2,128)S(1)}, f32[384,1,2]{0,2,1:T(2,128)S(1)}, f32[384,1,2,128]{0,3,2,1:T(8,128)S(1)}, bf16[12288,128]{0,1:T(8...) while((s32[]{:T(128)}, f32[384,1,2]{0,2,1:T(2,128)S(1)}, ...), condition=%wide.region_3.4_spmd.clone, body=%wide.region_0.3_spmd.clone.sunk | while | flops 312907648 | bytes 25586904 | solution.py:114
  189.6 3.3 %fusion.79 = f32[384,1,2,128]{0,3,2,1:T(8,128)S(1)} fusion(f32[2,1024,384]{2,1,0:T(8,128)} %get-tuple-element.251, f32[384,2]{0,1:T(2,128)S(1)} %bitcast.199, pred[384,1024]{0,1:T(8,128)(4,1)S(1)} %broadcast_compare_fusion.2, f32[384,1,2,128]{0,3,2,1:T(8,128)S(1)} %get-tuple-element.268, bf16[12288,128]{0,1:T(8,128)(2,1)} %get-tuple-element.283, ...), kind=kOutput, calls=%fused_computation.13.clone.1 | convolution fusion | flops 205553664 | bytes 4593669 | tf_op jit(solution)/shard_map/while/body/eval_jaxpr/ihcj,jhe->ihce/dot_general | solution.py:92
  197.5 3.4 %fusion.79 = f32[384,1,2,128]{0,3,2,1:T(8,128)S(1)} fusion(f32[2,1024,384]{2,1,0:T(8,128)} %get-tuple-element.251, f32[384,2]{0,1:T(2,128)S(1)} %bitcast.199, pred[384,1024]{0,1:T(8,128)(4,1)S(1)} %broadcast_compare_fusion.2, f32[384,1,2,128]{0,3,2,1:T(8,128)S(1)} %get-tuple-element.268, bf16[12288,128]{0,1:T(8,128)(2,1)} %get-tuple-element.283, ...), kind=kOutput, calls=%fused_computation.13.clone.1 | convolution fusion | flops 205553664 | bytes 4593669 | tf_op jit(solution)/shard_map/while/body/eval_jaxpr/ihcj,jhe->ihce/dot_general | solution.py:92
  205.5 3.2 %fusion.79 = f32[384,1,2,128]{0,3,2,1:T(8,128)S(1)} fusion(f32[2,1024,384]{2,1,0:T(8,128)} %get-tuple-element.251, f32[384,2]{0,1:T(2,128)S(1)} %bitcast.199, pred[384,1024]{0,1:T(8,128)(4,1)S(1)} %broadcast_compare_fusion.2, f32[384,1,2,128]{0,3,2,1:T(8,128)S(1)} %get-tuple-element.268, bf16[12288,128]{0,1:T(8,128)(2,1)} %get-tuple-element.283, ...), kind=kOutput, calls=%fused_computation.13.clone.1 | convolution fusion | flops 205553664 | bytes 4593669 | tf_op jit(solution)/shard_map/while/body/eval_jaxpr/ihcj,jhe->ihce/dot_general | solution.py:92
  213.3 3.2 %fusion.79 = f32[384,1,2,128]{0,3,2,1:T(8,128)S(1)} fusion(f32[2,1024,384]{2,1,0:T(8,128)} %get-tuple-element.251, f32[384,2]{0,1:T(2,128)S(1)} %bitcast.199, pred[384,1024]{0,1:T(8,128)(4,1)S(1)} %broadcast_compare_fusion.2, f32[384,1,2,128]{0,3,2,1:T(8,128)S(1)} %get-tuple-element.268, bf16[12288,128]{0,1:T(8,128)(2,1)} %get-tuple-element.283, ...), kind=kOutput, calls=%fused_computation.13.clone.1 | convolution fusion | flops 205553664 | bytes 4593669 | tf_op jit(solution)/shard_map/while/body/eval_jaxpr/ihcj,jhe->ihce/dot_general | solution.py:92
  221.2 3.2 %fusion.79 = f32[384,1,2,128]{0,3,2,1:T(8,128)S(1)} fusion(f32[2,1024,384]{2,1,0:T(8,128)} %get-tuple-element.251, f32[384,2]{0,1:T(2,128)S(1)} %bitcast.199, pred[384,1024]{0,1:T(8,128)(4,1)S(1)} %broadcast_compare_fusion.2, f32[384,1,2,128]{0,3,2,1:T(8,128)S(1)} %get-tuple-element.268, bf16[12288,128]{0,1:T(8,128)(2,1)} %get-tuple-element.283, ...), kind=kOutput, calls=%fused_computation.13.clone.1 | convolution fusion | flops 205553664 | bytes 4593669 | tf_op jit(solution)/shard_map/while/body/eval_jaxpr/ihcj,jhe->ihce/dot_general | solution.py:92
  229.1 3.2 %fusion.79 = f32[384,1,2,128]{0,3,2,1:T(8,128)S(1)} fusion(f32[2,1024,384]{2,1,0:T(8,128)} %get-tuple-element.251, f32[384,2]{0,1:T(2,128)S(1)} %bitcast.199, pred[384,1024]{0,1:T(8,128)(4,1)S(1)} %broadcast_compare_fusion.2, f32[384,1,2,128]{0,3,2,1:T(8,128)S(1)} %get-tuple-element.268, bf16[12288,128]{0,1:T(8,128)(2,1)} %get-tuple-element.283, ...), kind=kOutput, calls=%fused_computation.13.clone.1 | convolution fusion | flops 205553664 | bytes 4593669 | tf_op jit(solution)/shard_map/while/body/eval_jaxpr/ihcj,jhe->ihce/dot_general | solution.py:92
  236.9 3.2 %fusion.79 = f32[384,1,2,128]{0,3,2,1:T(8,128)S(1)} fusion(f32[2,1024,384]{2,1,0:T(8,128)} %get-tuple-element.251, f32[384,2]{0,1:T(2,128)S(1)} %bitcast.199, pred[384,1024]{0,1:T(8,128)(4,1)S(1)} %broadcast_compare_fusion.2, f32[384,1,2,128]{0,3,2,1:T(8,128)S(1)} %get-tuple-element.268, bf16[12288,128]{0,1:T(8,128)(2,1)} %get-tuple-element.283, ...), kind=kOutput, calls=%fused_computation.13.clone.1 | convolution fusion | flops 205553664 | bytes 4593669 | tf_op jit(solution)/shard_map/while/body/eval_jaxpr/ihcj,jhe->ihce/dot_general | solution.py:92
  244.8 3.2 %fusion.79 = f32[384,1,2,128]{0,3,2,1:T(8,128)S(1)} fusion(f32[2,1024,384]{2,1,0:T(8,128)} %get-tuple-element.251, f32[384,2]{0,1:T(2,128)S(1)} %bitcast.199, pred[384,1024]{0,1:T(8,128)(4,1)S(1)} %broadcast_compare_fusion.2, f32[384,1,2,128]{0,3,2,1:T(8,128)S(1)} %get-tuple-element.268, bf16[12288,128]{0,1:T(8,128)(2,1)} %get-tuple-element.283, ...), kind=kOutput, calls=%fused_computation.13.clone.1 | convolution fusion | flops 205553664 | bytes 4593669 | tf_op jit(solution)/shard_map/while/body/eval_jaxpr/ihcj,jhe->ihce/dot_general | solution.py:92
  260.7 5.9 %all-to-all-start.1 = ((bf16[32,1,16,256]{3,2,1,0:T(8,128)(2,1)}), bf16[32,1,16,256]{3,2,1,0:T(8,128)(2,1)S(1)}, u32[]{:S(2)}, u32[]{:S(2)}) async-start(bf16[32,1,16,256]{3,2,1,0:T(8,128)(2,1)} %fusion.48), calls=%async_computation.1 | async-start | bytes 524288 | tf_op jit(solution)/shard_map/all_to_all | solution.py:166
  266.7 21.0 %all-to-all-done.1 = bf16[32,1,16,256]{3,2,1,0:T(8,128)(2,1)S(1)} async-done(((bf16[32,1,16,256]{3,2,1,0:T(8,128)(2,1)}), bf16[32,1,16,256]{3,2,1,0:T(8,128)(2,1)S(1)}, u32[]{:S(2)}, u32[]{:S(2)}) %all-to-all-start.1) | async-done | bytes 262176 | tf_op jit(solution)/shard_map/all_to_all | solution.py:166
  290.0 16.2 %all-gather.6.cloned.1.call-done = bf16[1,1,384,2048]{2,3,1,0:T(8,128)(2,1)} async-done(((bf16[1,1,384,128]{2,3,1,0:T(8,128)(2,1)}), bf16[1,1,384,2048]{2,3,1,0:T(8,128)(2,1)}) %all-gather.6.cloned.1.call-update) | async-done | bytes 1572880 | tf_op jit(solution)/shard_map/all_gather | solution.py:152
  (238 shorter events, 118.4 us)
Async XLA Ops:
  7.2 250.5 %copy-start = (bf16[1,2048,256]{2,1,0:T(8,128)(2,1)S(1)}, bf16[1,2048,256]{2,1,0:T(8,128)(2,1)}, u32[]{:S(2)}) copy-start(bf16[1,2048,256]{2,1,0:T(8,128)(2,1)} %param.27) | copy-start | bytes 3145732
  7.2 59.3 %copy-start.3 = (bf16[384,128]{1,0:T(8,128)(2,1)S(1)}, bf16[384,128]{1,0:T(8,128)(2,1)}, u32[]{:S(2)}) copy-start(bf16[384,128]{1,0:T(8,128)(2,1)} %param.15) | copy-start | bytes 294916
  7.2 148.9 %all-gather.4.cloned.1.call-start = ((), (), s32[]{:S(2)}) async-start(), calls=%async_computation.2 | async-start | bytes 6488064 | tf_op jit(solution)/shard_map/all_gather | solution.py:41
  10.1 247.6 %all-gather.8.cloned.1.call-start = ((), (), s32[]{:S(2)}) async-start(), calls=%async_computation.4 | async-start | bytes 2228224 | tf_op jit(solution)/shard_map/all_gather | solution.py:161
  57.0 12.1 %collective-permute-start = (bf16[32,1,16,256]{3,2,1,0:T(8,128)(2,1)S(1)}, bf16[32,1,16,256]{3,2,1,0:T(8,128)(2,1)S(1)}, u32[]{:S(2)}, u32[]{:S(2)}) collective-permute-start(bf16[32,1,16,256]{3,2,1,0:T(8,128)(2,1)S(1)} %all_to_all.10), channel_id=1, source_target_pairs={{0,1},{1,2},{2,3},{3,4},{4,5},{5,6},{6,7},{7,8},{8,9},{9,10},{10,1... | collective-permute-start | bytes 786440 | tf_op jit(solution)/shard_map/ppermute | solution.py:24
  60.4 10.7 %collective-permute-start.1 = (bf16[32,1,16,256]{3,2,1,0:T(8,128)(2,1)S(1)}, bf16[32,1,16,256]{3,2,1,0:T(8,128)(2,1)S(1)}, u32[]{:S(2)}, u32[]{:S(2)}) collective-permute-start(bf16[32,1,16,256]{3,2,1,0:T(8,128)(2,1)S(1)} %all_to_all.10), channel_id=1, source_target_pairs={{0,15},{1,0},{2,1},{3,2},{4,3},{5,4},{6,5},{7,6},{8,7},{9,8},{10,9... | collective-permute-start | bytes 786440 | tf_op jit(solution)/shard_map/ppermute | solution.py:29
  69.1 11.6 %collective-permute-start.2 = (bf16[32,1,16,256]{3,2,1,0:T(8,128)(2,1)S(1)}, bf16[32,1,16,256]{3,2,1,0:T(8,128)(2,1)S(1)}, u32[]{:S(2)}, u32[]{:S(2)}) collective-permute-start(bf16[32,1,16,256]{3,2,1,0:T(8,128)(2,1)S(1)} %collective-permute-done), channel_id=1, source_target_pairs={{0,1},{1,2},{2,3},{3,4},{4,5},{5,6},{6,7},{7,8},{8,9},{9,10},{10,1... | collective-permute-start | bytes 786440 | tf_op jit(solution)/shard_map/ppermute | solution.py:24
  71.0 11.6 %collective-permute-start.3 = (bf16[32,1,16,256]{3,2,1,0:T(8,128)(2,1)S(1)}, bf16[32,1,16,256]{3,2,1,0:T(8,128)(2,1)S(1)}, u32[]{:S(2)}, u32[]{:S(2)}) collective-permute-start(bf16[32,1,16,256]{3,2,1,0:T(8,128)(2,1)S(1)} %collective-permute-done.1), channel_id=1, source_target_pairs={{0,15},{1,0},{2,1},{3,2},{4,3},{5,4},{6,5},{7,6},{8,7},{9,8},{10,9... | collective-permute-start | bytes 786440 | tf_op jit(solution)/shard_map/ppermute | solution.py:29
  80.7 11.6 %collective-permute-start.4 = (bf16[32,1,16,256]{3,2,1,0:T(8,128)(2,1)S(1)}, bf16[32,1,16,256]{3,2,1,0:T(8,128)(2,1)S(1)}, u32[]{:S(2)}, u32[]{:S(2)}) collective-permute-start(bf16[32,1,16,256]{3,2,1,0:T(8,128)(2,1)S(1)} %collective-permute-done.2), channel_id=1, source_target_pairs={{0,1},{1,2},{2,3},{3,4},{4,5},{5,6},{6,7},{7,8},{8,9},{9,10},{10,1... | collective-permute-start | bytes 786440 | tf_op jit(solution)/shard_map/ppermute | solution.py:24
  82.6 11.6 %collective-permute-start.5 = (bf16[32,1,16,256]{3,2,1,0:T(8,128)(2,1)S(1)}, bf16[32,1,16,256]{3,2,1,0:T(8,128)(2,1)S(1)}, u32[]{:S(2)}, u32[]{:S(2)}) collective-permute-start(bf16[32,1,16,256]{3,2,1,0:T(8,128)(2,1)S(1)} %collective-permute-done.3), channel_id=1, source_target_pairs={{0,15},{1,0},{2,1},{3,2},{4,3},{5,4},{6,5},{7,6},{8,7},{9,8},{10,9... | collective-permute-start | bytes 786440 | tf_op jit(solution)/shard_map/ppermute | solution.py:29
  92.3 11.6 %collective-permute-start.6 = (bf16[32,1,16,256]{3,2,1,0:T(8,128)(2,1)S(1)}, bf16[32,1,16,256]{3,2,1,0:T(8,128)(2,1)S(1)}, u32[]{:S(2)}, u32[]{:S(2)}) collective-permute-start(bf16[32,1,16,256]{3,2,1,0:T(8,128)(2,1)S(1)} %collective-permute-done.4), channel_id=1, source_target_pairs={{0,1},{1,2},{2,3},{3,4},{4,5},{5,6},{6,7},{7,8},{8,9},{9,10},{10,1... | collective-permute-start | bytes 786440 | tf_op jit(solution)/shard_map/ppermute | solution.py:24
  94.2 11.6 %collective-permute-start.7 = (bf16[32,1,16,256]{3,2,1,0:T(8,128)(2,1)S(1)}, bf16[32,1,16,256]{3,2,1,0:T(8,128)(2,1)S(1)}, u32[]{:S(2)}, u32[]{:S(2)}) collective-permute-start(bf16[32,1,16,256]{3,2,1,0:T(8,128)(2,1)S(1)} %collective-permute-done.5), channel_id=1, source_target_pairs={{0,15},{1,0},{2,1},{3,2},{4,3},{5,4},{6,5},{7,6},{8,7},{9,8},{10,9... | collective-permute-start | bytes 786440 | tf_op jit(solution)/shard_map/ppermute | solution.py:29
  103.8 11.6 %collective-permute-start.8 = (bf16[32,1,16,256]{3,2,1,0:T(8,128)(2,1)S(1)}, bf16[32,1,16,256]{3,2,1,0:T(8,128)(2,1)S(1)}, u32[]{:S(2)}, u32[]{:S(2)}) collective-permute-start(bf16[32,1,16,256]{3,2,1,0:T(8,128)(2,1)S(1)} %collective-permute-done.6), channel_id=1, source_target_pairs={{0,1},{1,2},{2,3},{3,4},{4,5},{5,6},{6,7},{7,8},{8,9},{9,10},{10,1... | collective-permute-start | bytes 786440 | tf_op jit(solution)/shard_map/ppermute | solution.py:24
  105.8 11.6 %collective-permute-start.9 = (bf16[32,1,16,256]{3,2,1,0:T(8,128)(2,1)S(1)}, bf16[32,1,16,256]{3,2,1,0:T(8,128)(2,1)S(1)}, u32[]{:S(2)}, u32[]{:S(2)}) collective-permute-start(bf16[32,1,16,256]{3,2,1,0:T(8,128)(2,1)S(1)} %collective-permute-done.7), channel_id=1, source_target_pairs={{0,15},{1,0},{2,1},{3,2},{4,3},{5,4},{6,5},{7,6},{8,7},{9,8},{10,9... | collective-permute-start | bytes 786440 | tf_op jit(solution)/shard_map/ppermute | solution.py:29
  113.0 39.5 %copy-start.6 = (bf16[1,4096,128]{2,1,0:T(8,128)(2,1)S(1)}, bf16[1,4096,128]{2,1,0:T(8,128)(2,1)}, u32[]{:S(2)}) copy-start(bf16[1,4096,128]{2,1,0:T(8,128)(2,1)} %param.25) | copy-start | bytes 3145732
  115.4 11.7 %collective-permute-start.10 = (bf16[32,1,16,256]{3,2,1,0:T(8,128)(2,1)S(1)}, bf16[32,1,16,256]{3,2,1,0:T(8,128)(2,1)S(1)}, u32[]{:S(2)}, u32[]{:S(2)}) collective-permute-start(bf16[32,1,16,256]{3,2,1,0:T(8,128)(2,1)S(1)} %collective-permute-done.8), channel_id=1, source_target_pairs={{0,1},{1,2},{2,3},{3,4},{4,5},{5,6},{6,7},{7,8},{8,9},{9,10},{10,1... | collective-permute-start | bytes 786440 | tf_op jit(solution)/shard_map/ppermute | solution.py:24
  117.3 11.7 %collective-permute-start.11 = (bf16[32,1,16,256]{3,2,1,0:T(8,128)(2,1)S(1)}, bf16[32,1,16,256]{3,2,1,0:T(8,128)(2,1)S(1)}, u32[]{:S(2)}, u32[]{:S(2)}) collective-permute-start(bf16[32,1,16,256]{3,2,1,0:T(8,128)(2,1)S(1)} %collective-permute-done.9), channel_id=1, source_target_pairs={{0,15},{1,0},{2,1},{3,2},{4,3},{5,4},{6,5},{7,6},{8,7},{9,8},{10,9... | collective-permute-start | bytes 786440 | tf_op jit(solution)/shard_map/ppermute | solution.py:29
  127.1 12.9 %collective-permute-start.12 = (bf16[32,1,16,256]{3,2,1,0:T(8,128)(2,1)S(1)}, bf16[32,1,16,256]{3,2,1,0:T(8,128)(2,1)S(1)}, u32[]{:S(2)}, u32[]{:S(2)}) collective-permute-start(bf16[32,1,16,256]{3,2,1,0:T(8,128)(2,1)S(1)} %collective-permute-done.10), channel_id=1, source_target_pairs={{0,1},{1,2},{2,3},{3,4},{4,5},{5,6},{6,7},{7,8},{8,9},{9,10},{10,1... | collective-permute-start | bytes 786440 | tf_op jit(solution)/shard_map/ppermute | solution.py:24
  129.1 12.9 %collective-permute-start.13 = (bf16[32,1,16,256]{3,2,1,0:T(8,128)(2,1)S(1)}, bf16[32,1,16,256]{3,2,1,0:T(8,128)(2,1)S(1)}, u32[]{:S(2)}, u32[]{:S(2)}) collective-permute-start(bf16[32,1,16,256]{3,2,1,0:T(8,128)(2,1)S(1)} %collective-permute-done.11), channel_id=1, source_target_pairs={{0,15},{1,0},{2,1},{3,2},{4,3},{5,4},{6,5},{7,6},{8,7},{9,8},{10,9... | collective-permute-start | bytes 786440 | tf_op jit(solution)/shard_map/ppermute | solution.py:29
  140.0 11.6 %collective-permute-start.14 = (bf16[32,1,16,256]{3,2,1,0:T(8,128)(2,1)S(1)}, bf16[32,1,16,256]{3,2,1,0:T(8,128)(2,1)S(1)}, u32[]{:S(2)}, u32[]{:S(2)}) collective-permute-start(bf16[32,1,16,256]{3,2,1,0:T(8,128)(2,1)S(1)} %collective-permute-done.12), channel_id=1, source_target_pairs={{0,1},{1,2},{2,3},{3,4},{4,5},{5,6},{6,7},{7,8},{8,9},{9,10},{10,1... | collective-permute-start | bytes 786440 | tf_op jit(solution)/shard_map/ppermute | solution.py:24
  155.9 150.3 %all-gather.6.cloned.1.call-start = ((), (), s32[]{:S(2)}) async-start(), calls=%async_computation.3 | async-start | bytes 1671168 | tf_op jit(solution)/shard_map/all_gather | solution.py:152
  162.3 94.6 %copy-start.5 = (f32[128]{0:T(128)S(1)}, f32[128]{0:T(128)}, u32[]{:S(2)}) copy-start(f32[128]{0:T(128)} %param.19) | copy-start | bytes 1540
  256.8 49.4 %copy-start.2 = (bf16[2048,256]{1,0:T(8,128)(2,1)S(1)}, bf16[2048,256]{1,0:T(8,128)(2,1)}, u32[]{:S(2)}) copy-start(bf16[2048,256]{1,0:T(8,128)(2,1)} %param.20) | copy-start | bytes 3145732
  260.7 27.0 %all-to-all-start.1 = ((bf16[32,1,16,256]{3,2,1,0:T(8,128)(2,1)}), bf16[32,1,16,256]{3,2,1,0:T(8,128)(2,1)S(1)}, u32[]{:S(2)}, u32[]{:S(2)}) async-start(bf16[32,1,16,256]{3,2,1,0:T(8,128)(2,1)} %fusion.48), calls=%async_computation.1 | async-start | bytes 524288 | tf_op jit(solution)/shard_map/all_to_all | solution.py:166
  (15 other events, 89.9 us)
Sparse Core Ops, SparseCore 0:
  10.6 88.9 all-gather.3
  156.0 51.7 all-gather.7
  257.8 48.3 all-gather.5
